TPU v7x, 512 devices: a whole 4x4x16 slice. The times are simulated.
512 devices in a mesh: sp: 16 (over z), tp: 4 (over y), dp: 8 (over x, core).
Axes of the slice: x: 4, y: 4, z: 16, core: 2. Of those that a mesh axis runs over, the one named last changes fastest.
Arguments:
- latent: bfloat16 [32768, 2048], P(('dp', 'sp', 'tp')), parts along dimension 0, may hold values from -6 to 6
- context: bfloat16 [2048, 2048], P(('dp', 'sp')), parts along dimension 0, may hold values from -6 to 6
- cond: bfloat16 [16384], P(('dp', 'sp')), parts along dimension 0, may hold values from -6 to 6
- context_cond: bfloat16 [2048], P('sp'), may hold values from -6 to 6
- norm_gain: float32 [2048], replicated, may hold values from 0.1 to 1.9
- mod_shift: bfloat16 [2048, 2048], P('sp', 'tp'), may hold values from -0.125 to 0.125
- mod_scale: bfloat16 [2048, 2048], P('sp', 'tp'), may hold values from -0.125 to 0.125
- mod_gate: bfloat16 [2048, 2048], P('sp', 'tp'), may hold values from -0.125 to 0.125
- w_query: bfloat16 [2048, 1024], P(None, 'tp'), may hold values from -0.125 to 0.125
- w_key: bfloat16 [2048, 1024], P(None, 'tp'), may hold values from -0.125 to 0.125
- w_value: bfloat16 [2048, 1024], P(None, 'tp'), may hold values from -0.125 to 0.125
- query_gain: float32 [64], replicated, may hold values from 1.4 to 2.2
- key_gain: float32 [64], replicated, may hold values from 0.1 to 1.9
- mix_lambda: float32 [8], P('tp'), may hold values from 0.3 to 0.8
- context_lift: float32 [8], P('tp'), may hold values from 1.5 to 2.5
- value_gain: float32 [128], replicated, may hold values from 0.1 to 1.9
- w_out: bfloat16 [1024, 2048], P('tp'), may hold values from -0.1875 to 0.1875
Outputs:
- output: bfloat16 [32768, 2048], P(('dp', 'sp', 'tp')), parts along dimension 0
There are 8 independent parts, one for each index of `dp`. A program takes and returns all parts, laid end to end along the dimension named above; an argument that names none is the same for every part. Nothing has to cross between parts.
All inputs are finite; a program needn't handle non-finite values.
Results may differ from a plain program's by a relative error of at most 0.006.
Values may be sent and summed in bfloat16 or wider, within the bound.
A program may use at most 64 MiB of HBM per device.

v0:
```python
import jax
import jax.numpy as jnp
from jax import lax
from jax.sharding import PartitionSpec as P

GRID = 64
token_eps = 0.01
head_eps = 0.001
rope_base = 10000.0
head_factor = 0.8
key_block = 512


def copy_for_each(array, axis):
    copies = jnp.broadcast_to(array, (lax.axis_size(axis), *array.shape))
    return lax.all_to_all(copies, axis, split_axis=0, concat_axis=0, tiled=True)


def taken_together(array, axis):
    return copy_for_each(array, axis).sum(axis=0)


def in_order(tiles, dim):
    tiles = jnp.moveaxis(tiles, 0, dim)
    shape = tiles.shape
    return tiles.reshape(*shape[:dim], shape[dim] * shape[dim + 1], *shape[dim + 2 :])


def collect(array, axis, dim):
    tiles = copy_for_each(array, axis)
    return in_order(tiles, dim)


def sent_together(arrays, axis, dim, along):
    both = jnp.concatenate(arrays, axis=along)
    out, at, gathered = (lax.all_gather(both, axis, axis=dim, tiled=True), 0, [])
    for a in arrays:
        gathered.append(lax.slice_in_dim(out, at, at + a.shape[along], axis=along))
        at += a.shape[along]
    return tuple(gathered)


def cut_along(array, dim, devices):
    before, after = (array.shape[:dim], array.shape[dim + 1 :])
    return jnp.moveaxis(array.reshape(*before, devices, -1, *after), dim, 0)


def sum_at_owner(array, axis, dim):
    devices = lax.axis_size(axis)
    tiles = lax.all_to_all(cut_along(array, dim, devices), axis, 0, 0, tiled=True)
    return jnp.sum(tiles, axis=0)


def modulated_norm(row_block, gain_vector, shift_vector, scale_vector):
    values = row_block.astype(jnp.float32)
    inverse = lax.rsqrt(jnp.mean(values * values, axis=-1, keepdims=True) + token_eps)
    return (values * inverse * gain_vector * (1.0 + scale_vector) + shift_vector).astype(
        jnp.bfloat16
    )


def head_norm(values, gain_vector):
    inverse = lax.rsqrt(jnp.mean(values * values, axis=-1, keepdims=True) + token_eps)
    return values * inverse * gain_vector


def rotate(values, positions):
    quarter = values.shape[-1] // 4
    inverse = rope_base ** (-jnp.arange(quarter, dtype=jnp.float32) / quarter)
    grid_row = (positions // GRID).astype(jnp.float32)
    grid_col = (positions % GRID).astype(jnp.float32)
    angles = jnp.stack([grid_row[:, None] * inverse, grid_col[:, None] * inverse], axis=1)
    cosine_table = jnp.cos(angles)[:, None, None]
    sine_table = jnp.sin(angles)[:, None, None]
    halves = values.reshape(values.shape[:3] + (2, 2, quarter))
    front_half = halves[..., 0, :]
    back_half = halves[..., 1, :]
    turned = jnp.stack(
        [
            front_half * cosine_table - back_half * sine_table,
            back_half * cosine_table + front_half * sine_table,
        ],
        axis=-2,
    )
    return turned.reshape(values.shape)


def project_heads(row_block, weight, gain_vector, positions, factor):
    row_count = row_block.shape[0]
    head_width = gain_vector.shape[0]
    product = jnp.dot(row_block, weight, preferred_element_type=jnp.float32)
    shaped = head_norm(product.reshape(row_count, -1, 2, head_width), gain_vector)
    if positions is not None:
        shaped = rotate(shaped, positions)
    return (shaped * factor).astype(jnp.bfloat16).reshape(row_count, -1)


def accumulate(running, queries, key_slab, value_slab, lift_rows):
    numerator, totals = running
    head_count = lift_rows.shape[0]
    head_width = queries.shape[1] // (2 * head_count)
    shaped_query = queries.reshape(queries.shape[0], head_count, 2, head_width)
    shaped_keys = key_slab.reshape(key_slab.shape[0], head_count, 2, head_width)
    shaped_values = value_slab.reshape(value_slab.shape[0], head_count, -1)
    scores = jnp.einsum(
        "qhmd,phmd->mhqp", shaped_query, shaped_keys, preferred_element_type=jnp.float32
    )
    weights = jnp.exp(scores + lift_rows[None, :, None, :])
    totals = totals + jnp.sum(weights, axis=-1)
    numerator = numerator + jnp.einsum(
        "mhqp,phe->mhqe",
        weights.astype(jnp.bfloat16),
        shaped_values,
        preferred_element_type=jnp.float32,
    )
    return (numerator, totals)


def accumulate_blocks(running, queries, key_slab, value_slab, lift_rows):
    row_count = key_slab.shape[0]
    full_blocks = row_count // key_block
    covered = full_blocks * key_block
    head_count = lift_rows.shape[0]
    slabs = (
        key_slab[:covered].reshape(full_blocks, key_block, -1),
        value_slab[:covered].reshape(full_blocks, key_block, -1),
        jnp.transpose(
            lift_rows[:, :covered].reshape(head_count, full_blocks, key_block), (1, 0, 2)
        ),
    )

    def scan_step(inside, slab):
        return (accumulate(inside, queries, slab[0], slab[1], slab[2]), None)

    running = lax.scan(scan_step, running, slabs)[0]
    running = accumulate(
        running, queries, key_slab[covered:], value_slab[covered:], lift_rows[:, covered:]
    )
    return running


def on_device(
    latent,
    context,
    cond,
    context_cond,
    norm_gain,
    mod_shift,
    mod_scale,
    mod_gate,
    w_query,
    w_key,
    w_value,
    query_gain,
    key_gain,
    mix_lambda,
    context_lift,
    value_gain,
    w_out,
):
    cond_act = jax.nn.silu(cond.astype(jnp.float32)).astype(jnp.bfloat16)
    context_act = jax.nn.silu(context_cond.astype(jnp.float32)).astype(jnp.bfloat16)
    both_acts = jnp.stack([cond_act, context_act])
    shifts = jnp.dot(both_acts, mod_shift, preferred_element_type=jnp.float32)
    scales = jnp.dot(both_acts, mod_scale, preferred_element_type=jnp.float32)
    gates = jnp.dot(cond_act[None, :], mod_gate, preferred_element_type=jnp.float32)
    partial_mod = jnp.concatenate([shifts, scales, gates], axis=0)
    summed = taken_together(partial_mod, "sp")
    modulation = collect(summed, "tp", 1)
    normed = modulated_norm(latent, norm_gain, modulation[0], modulation[2])
    context_normed = modulated_norm(context, norm_gain, modulation[1], modulation[3])
    local_rows = latent.shape[0]
    offset = lax.axis_index("sp") * (local_rows * lax.axis_size("tp"))
    head_width = query_gain.shape[0]
    pieces = lax.all_gather(normed, "tp", axis=0, tiled=True)
    positions = offset + jnp.arange(pieces.shape[0], dtype=jnp.int32)
    query_part = project_heads(pieces, w_query, query_gain, positions, head_width ** (-0.5))
    key_part = project_heads(pieces, w_key, key_gain, positions, 1.0)
    value_part = jnp.dot(pieces, w_value, preferred_element_type=jnp.float32).astype(jnp.bfloat16)
    projected = jnp.concatenate([query_part, key_part, value_part], axis=1)
    qk_width = w_query.shape[1]
    queries = projected[:, :qk_width]
    latent_keys = projected[:, qk_width : 2 * qk_width]
    latent_values = projected[:, 2 * qk_width :]
    heads_here = mix_lambda.shape[0]
    query_rows = queries.shape[0]
    value_width = latent_values.shape[1] // heads_here
    empty = (
        jnp.zeros((2, heads_here, query_rows, value_width), jnp.float32),
        jnp.zeros((2, heads_here, query_rows), jnp.float32),
    )
    latent_count = latent_keys.shape[0]
    own_keys = project_heads(context_normed, w_key, key_gain, None, 1.0)
    own_values = jnp.dot(context_normed, w_value, preferred_element_type=jnp.float32).astype(
        jnp.bfloat16
    )
    shard_keys = jnp.concatenate([latent_keys, own_keys], axis=0)
    shard_values = jnp.concatenate([latent_values, own_values], axis=0)
    extra_rows = own_keys.shape[0]
    shard_rows = latent_count + extra_rows
    pieces = sent_together((shard_keys, shard_values), "sp", 0, 1)
    row_index = jnp.arange(pieces[0].shape[0], dtype=jnp.int32) % shard_rows
    lift_rows = jnp.where(row_index[None, :] >= latent_count, context_lift[:, None], 0.0)
    numerator, totals = accumulate_blocks(empty, queries, pieces[0], pieces[1], lift_rows)
    ratios = numerator / totals[..., None]
    mixed_heads = ratios[0] - mix_lambda[:, None, None] * ratios[1]
    inverse = lax.rsqrt(jnp.mean(mixed_heads * mixed_heads, axis=-1, keepdims=True) + head_eps)
    head_out = (mixed_heads * inverse * value_gain * head_factor).astype(jnp.bfloat16)
    out_weight = w_out.reshape(heads_here, value_width, w_out.shape[1])
    mixture = sum_at_owner(
        jnp.einsum("hqe,hed->qd", head_out, out_weight, preferred_element_type=jnp.float32), "tp", 0
    )
    return (latent.astype(jnp.float32) + modulation[4] * mixture).astype(jnp.bfloat16)


def solution(mesh):
    placed = (
        P(("dp", "sp", "tp"), None),
        P(("dp", "sp"), None),
        P(("dp", "sp")),
        P("sp"),
        P(),
        P("sp", "tp"),
        P("sp", "tp"),
        P("sp", "tp"),
        P(None, "tp"),
        P(None, "tp"),
        P(None, "tp"),
        P(),
        P(),
        P("tp"),
        P("tp"),
        P(),
        P("tp", None),
    )
    return jax.shard_map(
        on_device,
        mesh=mesh,
        in_specs=placed,
        out_specs=P(("dp", "sp", "tp"), None),
        check_vma=False,
    )
```

profile of v0, /device:TPU:2, one launch (start us, length us, event | category | flops | bytes accessed | tf_op | source)
XLA Modules:
  0.0 231.5 jit_solution(1074336177027201900)
XLA Ops:
  7.4 1.1 fusion.33
  8.4 1.0 fusion.36
  9.5 1.0 fusion.37
  11.3 15.2 %all-to-all-start = ((f32[16,5,512]{2,1,0:T(8,128)}), f32[16,5,512]{2,1,0:T(8,128)}, u32[]{:S(2)}, u32[]{:S(2)}) async-start(f32[16,5,512]{2,1,0:T(8,128)} %broadcast_in_dim.21), calls=%async_computation | async-start | bytes 524288 | tf_op jit(solution)/shard_map/all_to_all | solution.py:16
  27.1 1.1 fusion.7
  28.7 16.2 %all-to-all-done = f32[16,5,512]{2,1,0:T(8,128)} async-done(((f32[16,5,512]{2,1,0:T(8,128)}), f32[16,5,512]{2,1,0:T(8,128)}, u32[]{:S(2)}, u32[]{:S(2)}) %all-to-all-start) | async-done | bytes 163872 | tf_op jit(solution)/shard_map/all_to_all | solution.py:16
  45.0 1.0 reduce_sum.90
  46.6 4.5 %all-to-all-start.1 = ((f32[4,5,512]{2,1,0:T(8,128)}), f32[4,5,512]{2,1,0:T(8,128)S(1)}, u32[]{:S(2)}, u32[]{:S(2)}) async-start(f32[4,5,512]{2,1,0:T(8,128)} %broadcast_in_dim.22), calls=%async_computation.1 | async-start | bytes 131072 | tf_op jit(solution)/shard_map/all_to_all | solution.py:16
  51.6 1.3 mul.366
  52.9 1.3 mul.331
  55.6 1.1 all-to-all-done.1
  57.3 1.5 fusion.11
  60.5 1.6 fusion.45
  62.7 1.3 multiply_convert_fusion.1
  64.1 1.5 convolution_convert_fusion.1
  65.6 19.4 %all-gather.3.cloned.1.call-done = bf16[256,2048]{1,0:T(8,128)(2,1)} async-done(((bf16[64,2048]{1,0:T(8,128)(2,1)}), bf16[256,2048]{1,0:T(8,128)(2,1)}) %all-gather.3.cloned.1.call-update) | async-done | bytes 1048592 | tf_op jit(solution)/shard_map/all_gather | solution.py:175
  85.0 2.2 bitcast_reduce_fusion.1
  89.4 1.7 copy.89
  94.5 77.1 %all-gather.5.cloned.1.call-done = bf16[4352,512]{1,0:T(8,128)(2,1)} async-done(((bf16[272,512]{1,0:T(8,128)(2,1)}), bf16[4352,512]{1,0:T(8,128)(2,1)}) %all-gather.5.cloned.1.call-update) | async-done | bytes 4456464 | tf_op jit(solution)/shard_map/all_gather | solution.py:36
  171.6 1.0 fusion.41
  172.8 4.5 %fusion.42 = (bf16[4096,256]{1,0:T(8,128)(2,1)}, bf16[4096,256]{1,0:T(8,128)(2,1)}) fusion(bf16[4352,512]{1,0:T(8,128)(2,1)} %all-gather.5.cloned.1.call-done), kind=kLoop, calls=%fused_computation.102 | loop fusion | bytes 8388608 | tf_op jit(solution)/shard_map/slice | solution.py:125
  177.3 21.7 %while.13 = (s32[]{:T(128)}, f32[2,2,256,128]{2,3,0,1:T(8,128)S(1)}, f32[2,2,256]{2,1,0:T(2,128)S(1)}, bf16[8,512,256]{2,1,0:T(8,128)(2,1)}, bf16[8,512,256]{2,1...) while((s32[]{:T(128)}, ...), condition=%wide.region_8.9_spmd.clone, body=%wide.region_6.8_spmd.clone.sunk | while | flops 203686912 | bytes 10125432 | solution.py:135
  177.3 1.1 constant_dynamic-slice_fusion.3
  180.0 1.1 constant_dynamic-slice_fusion.3
  182.8 1.1 constant_dynamic-slice_fusion.3
  185.5 1.1 constant_dynamic-slice_fusion.3
  188.2 1.1 constant_dynamic-slice_fusion.3
  190.9 1.1 constant_dynamic-slice_fusion.3
  193.6 1.1 constant_dynamic-slice_fusion.3
  196.3 1.1 constant_dynamic-slice_fusion.3
  200.6 21.3 %all_to_all.15 = f32[4,64,2048]{2,1,0:T(8,128)S(1)} all-to-all(f32[4,64,2048]{2,1,0:T(8,128)S(1)} %convolution_bitcast_fusion.1), channel_id=1, replica_groups=mesh['sp'=16,'tp'=4,'dp'=8] {'tp'}, dimensions={0} | all-to-all | bytes 4194304 | tf_op jit(solution)/shard_map/all_to_all | solution.py:50
  222.8 1.8 fusion.12
  (153 shorter events, 28.9 us)
Async XLA Ops:
  6.5 193.6 %copy-start = (bf16[256,2048]{1,0:T(8,128)(2,1)S(1)}, bf16[256,2048]{1,0:T(8,128)(2,1)}, u32[]{:S(2)}) copy-start(bf16[256,2048]{1,0:T(8,128)(2,1)} %param.35) | copy-start | bytes 3145732
  6.5 50.8 %copy-start.5 = (bf16[64,2048]{1,0:T(8,128)(2,1)S(1)}, bf16[64,2048]{1,0:T(8,128)(2,1)}, u32[]{:S(2)}) copy-start(bf16[64,2048]{1,0:T(8,128)(2,1)} %param.19) | copy-start | bytes 786436
  6.5 50.8 %copy-start.11 = (f32[2048]{0:T(1024)S(1)}, f32[2048]{0:T(1024)}, u32[]{:S(2)}) copy-start(f32[2048]{0:T(1024)} %param.23) | copy-start | bytes 24580
  6.5 53.8 %copy-start.6 = (bf16[16,2048]{1,0:T(8,128)(2,1)S(1)}, bf16[16,2048]{1,0:T(8,128)(2,1)}, u32[]{:S(2)}) copy-start(bf16[16,2048]{1,0:T(8,128)(2,1)} %param.20) | copy-start | bytes 196612
  6.5 54.0 %copy-start.2 = (bf16[2048,256]{1,0:T(8,128)(2,1)S(1)}, bf16[2048,256]{1,0:T(8,128)(2,1)}, u32[]{:S(2)}) copy-start(bf16[2048,256]{1,0:T(8,128)(2,1)} %param.28) | copy-start | bytes 3145732
  10.5 53.5 %copy-start.3 = (bf16[2048,256]{1,0:T(8,128)(2,1)S(1)}, bf16[2048,256]{1,0:T(8,128)(2,1)}, u32[]{:S(2)}) copy-start(bf16[2048,256]{1,0:T(8,128)(2,1)} %param.29) | copy-start | bytes 3145732
  11.3 33.7 %all-to-all-start = ((f32[16,5,512]{2,1,0:T(8,128)}), f32[16,5,512]{2,1,0:T(8,128)}, u32[]{:S(2)}, u32[]{:S(2)}) async-start(f32[16,5,512]{2,1,0:T(8,128)} %broadcast_in_dim.21), calls=%async_computation | async-start | bytes 524288 | tf_op jit(solution)/shard_map/all_to_all | solution.py:16
  46.6 10.1 %all-to-all-start.1 = ((f32[4,5,512]{2,1,0:T(8,128)}), f32[4,5,512]{2,1,0:T(8,128)S(1)}, u32[]{:S(2)}, u32[]{:S(2)}) async-start(f32[4,5,512]{2,1,0:T(8,128)} %broadcast_in_dim.22), calls=%async_computation.1 | async-start | bytes 131072 | tf_op jit(solution)/shard_map/all_to_all | solution.py:16
  51.0 34.0 %all-gather.3.cloned.1.call-start = ((), (), s32[]{:S(2)}) async-start(), calls=%async_computation.3 | async-start | bytes 1310720 | tf_op jit(solution)/shard_map/all_gather | solution.py:175
  57.3 6.8 %copy-start.12 = (f32[1,4,512]{2,0,1:T(1,128)S(1)}, f32[1,4,512]{2,0,1:T(1,128)}, u32[]{:S(2)}) copy-start(f32[1,4,512]{2,0,1:T(1,128)} %get-tuple-element.141) | copy-start | bytes 24580
  58.8 112.8 %all-gather.5.cloned.1.call-start = ((), (), s32[]{:S(2)}) async-start(), calls=%async_computation.4 | async-start | bytes 4734976 | tf_op jit(solution)/shard_map/all_gather | solution.py:36
  60.5 1.7 copy-start.19
  65.6 22.2 %copy-start.17 = (f32[2,2,16]{2,1,0:T(2,128)S(1)}, f32[2,2,16]{2,1,0:T(2,128)}, u32[]{:S(2)}) copy-start(f32[2,2,16]{2,1,0:T(2,128)} %mul.366) | copy-start | bytes 772
  65.6 22.3 %copy-start.16 = (f32[2,2,16]{2,1,0:T(2,128)S(1)}, f32[2,2,16]{2,1,0:T(2,128)}, u32[]{:S(2)}) copy-start(f32[2,2,16]{2,1,0:T(2,128)} %mul.331) | copy-start | bytes 772
  85.0 2.2 copy-start.1
  87.2 0.8 copy-start.9
  87.2 0.8 copy-start.10
  87.8 3.3 %copy-start.4 = (bf16[2048,256]{1,0:T(8,128)(2,1)S(1)}, bf16[2048,256]{1,0:T(8,128)(2,1)}, u32[]{:S(2)}) copy-start(bf16[2048,256]{1,0:T(8,128)(2,1)} %param.29) | copy-start | bytes 3145732
  87.9 3.7 %copy-start.13 = (bf16[16,256]{1,0:T(8,128)(2,1)S(1)}, bf16[16,256]{1,0:T(8,128)(2,1)}, u32[]{:S(2)}) copy-start(bf16[16,256]{1,0:T(8,128)(2,1)} %convolution_convert_fusion.1) | copy-start | bytes 24580
  87.9 3.7 %copy-start.15 = (bf16[16,256]{1,0:T(8,128)(2,1)S(1)}, bf16[16,256]{1,0:T(8,128)(2,1)}, u32[]{:S(2)}) copy-start(bf16[16,256]{1,0:T(8,128)(2,1)} %multiply_convert_fusion.1) | copy-start | bytes 24580
  91.1 0.9 copy-start.7
  93.6 83.8 %copy-start.8 = (f32[2,4352]{1,0:T(2,128)}, f32[2,4352]{1,0:T(2,128)S(1)}, u32[]{:S(2)}) copy-start(f32[2,4352]{1,0:T(2,128)S(1)} %broadcast_select_fusion) | copy-start | bytes 104452
  177.3 21.7 %slice-start = ((f32[2,4352]{1,0:T(2,128)}), f32[2,256]{1,0:T(2,128)S(1)}, s32[]{:S(2)}) async-start(f32[2,4352]{1,0:T(2,128)} %copy-done.8), calls=%async_computation.5 | async-start | bytes 4096 | tf_op jit(solution)/shard_map/slice | solution.py:137
  199.0 0.7 copy-start.18
  199.0 0.8 copy-start.20
  221.8 1.0 copy-start.14
Sparse Core Ops, SparseCore 0:
  58.9 26.0 all-gather.2
  92.9 78.6 all-gather.4
where the time goes:
time: 232 us; the launch traced here: 231 us
  waiting for transfers between devices  114 us (49%)
  local copies, waits for them, and re-layouts  24.7 us (11%)
  blocking collectives  21.3 us (9%)
  other arithmetic  19.8 us (9%)
  starting transfers between devices  19.8 us (9%)
  matrix products  17.8 us (8%)
  between operations  13.8 us (6%)
    all_gather x1, waiting for transfers between devices, sent_together(): lax.all_gather(both, axis, axis=dim, tiled=True)  77.1 us
    all_to_all x1, blocking collectives, sum_at_owner(): lax.all_to_all(cut_along(array, dim, devices), axis, 0, 0, tiled=True)  21.3 us
    all_to_all x2, starting transfers between devices, copy_for_each(): return lax.all_to_all(copies, axis, split_axis=0, concat_axis=0, tiled=True)  19.7 us
    all_gather x1, waiting for transfers between devices, on_device(): pieces = lax.all_gather(normed, 'tp', axis=0, tiled=True)  19.4 us
    all_to_all x2, waiting for transfers between devices, copy_for_each(): return lax.all_to_all(copies, axis, split_axis=0, concat_axis=0, tiled=True)  17.3 us
    dynamic_slice x24, local copies, waits for them, and re-layouts, accumulate_blocks(): running = lax.scan(scan_step, running, slabs)[0]  10.8 us
    dot_general x9, matrix products, accumulate(): jnp.einsum('qhmd,phmd->mhqp', shaped_query, shaped_keys, preferred_elemen...  4.96 us
  transfers between devices with their start and end apart: 4, of which 4 were waited for; matrix products, arithmetic and copies ran while one was open for 7% of the time, Pallas kernels for 0%

commit v1 on v0

--- a/solution.py
+++ b/solution.py
@@ -172,7 +172,24 @@
     local_rows = latent.shape[0]
     offset = lax.axis_index("sp") * (local_rows * lax.axis_size("tp"))
     head_width = query_gain.shape[0]
-    pieces = lax.all_gather(normed, "tp", axis=0, tiled=True)
+    size, position, rows = (lax.axis_size("tp"), lax.axis_index("tp"), normed.shape[0])
+    forward = [(i, (i + 1) % size) for i in range(size)]
+    left = [(i, (i - 1) % size) for i in range(size)]
+    out_2 = jnp.zeros((*normed.shape[:0], size * rows, *normed.shape[0 + 1 :]), normed.dtype)
+    out_2 = lax.dynamic_update_slice_in_dim(out_2, normed, position * rows, axis=0)
+    from_left = from_right = normed
+    half = size // 2
+    for step in range(1, half + 1):
+        from_left = lax.ppermute(from_left, "tp", forward)
+        out_2 = lax.dynamic_update_slice_in_dim(
+            out_2, from_left, (position - step) % size * rows, axis=0
+        )
+        if step < size - half:
+            from_right = lax.ppermute(from_right, "tp", left)
+            out_2 = lax.dynamic_update_slice_in_dim(
+                out_2, from_right, (position + step) % size * rows, axis=0
+            )
+    pieces = out_2
     positions = offset + jnp.arange(pieces.shape[0], dtype=jnp.int32)
     query_part = project_heads(pieces, w_query, query_gain, positions, head_width ** (-0.5))
     key_part = project_heads(pieces, w_key, key_gain, positions, 1.0)

time: 232 us -> 268 us (1.16)
  matrix products: 17.8 us -> 44.2 us
  local copies, waits for them, and re-layouts: 24.7 us -> 46 us
  waiting for transfers between devices: 114 us -> 95.1 us
  starting transfers between devices: 19.8 us -> 28.6 us
  other arithmetic: 19.8 us -> 16.4 us
    all_gather x1 -> x0, waiting for transfers between devices: 19.4 us -> none  [on_device(): pieces = lax.all_gather(normed, 'tp', axis=0, tiled=True)]
    dot_general x9, matrix products: 3.01 us -> 21.6 us  [accumulate(): jnp.einsum('mhqp,phe->mhqe', weights.astype(jnp.bfloat16), shaped_values,...]
    dynamic_slice x24, local copies, waits for them, and re-layouts: 10.8 us -> 24 us  [accumulate_blocks(): running = lax.scan(scan_step, running, slabs)[0]]
    ppermute x0 -> x3, starting transfers between devices: none -> 8.96 us  [the longest x1 4.58 us: on_device(): from_right = lax.ppermute(from_right, 'tp', left)]
    dot_general x9, matrix products: 4.96 us -> 13.7 us  [accumulate(): jnp.einsum('qhmd,phmd->mhqp', shaped_query, shaped_keys, preferred_elemen...]
    all_gather x1, waiting for transfers between devices: 77.1 us -> 70 us  [sent_together(): lax.all_gather(both, axis, axis=dim, tiled=True)]
    ppermute x0 -> x3, waiting for transfers between devices: none -> 6.53 us  [the longest x2 6.53 us: on_device(): from_left = lax.ppermute(from_left, 'tp', forward)]
    add x8, local copies, waits for them, and re-layouts: 0.05 us -> 5.47 us  [accumulate(): weights = jnp.exp(scores + lift_rows[None, :, None, :])]
  transfers between devices with their start and end apart: 4 -> 6, of which waited for: 4 -> 4; matrix products, arithmetic and copies ran while one was open for 7% -> 6% of each run, Pallas kernels for 0% -> 0%
where the time goes in v1:
time: 268 us; the launch traced here: 266 us
  waiting for transfers between devices  95.1 us (35%)
  local copies, waits for them, and re-layouts  46 us (17%)
  matrix products  44.2 us (16%)
  starting transfers between devices  28.6 us (11%)
  blocking collectives  21.2 us (8%)
  other arithmetic  16.4 us (6%)
  between operations  13.9 us (5%)
    all_gather x1, waiting for transfers between devices, sent_together(): lax.all_gather(both, axis, axis=dim, tiled=True)  70 us
    dynamic_slice x24, local copies, waits for them, and re-layouts, accumulate_blocks(): running = lax.scan(scan_step, running, slabs)[0]  24 us
    dot_general x9, matrix products, accumulate(): jnp.einsum('mhqp,phe->mhqe', weights.astype(jnp.bfloat16), shaped_values,...  21.6 us
    all_to_all x1, blocking collectives, sum_at_owner(): lax.all_to_all(cut_along(array, dim, devices), axis, 0, 0, tiled=True)  21.2 us
    all_to_all x2, starting transfers between devices, copy_for_each(): return lax.all_to_all(copies, axis, split_axis=0, concat_axis=0, tiled=True)  19.7 us
    all_to_all x2, waiting for transfers between devices, copy_for_each(): return lax.all_to_all(copies, axis, split_axis=0, concat_axis=0, tiled=True)  18.5 us
    dot_general x9, matrix products, accumulate(): jnp.einsum('qhmd,phmd->mhqp', shaped_query, shaped_keys, preferred_elemen...  13.7 us
    ppermute x2, waiting for transfers between devices, on_device(): from_left = lax.ppermute(from_left, 'tp', forward)  6.53 us
  transfers between devices with their start and end apart: 6, of which 4 were waited for; matrix products, arithmetic and copies ran while one was open for 6% of the time, Pallas kernels for 0%

profile of v1, /device:TPU:2, one launch (start us, length us, event | category | flops | bytes accessed | tf_op | source)
XLA Modules:
  0.0 265.8 jit_solution(3963134892507198432)
XLA Ops:
  11.3 15.2 %all-to-all-start = ((f32[16,5,512]{2,1,0:T(8,128)}), f32[16,5,512]{2,1,0:T(8,128)S(1)}, u32[]{:S(2)}, u32[]{:S(2)}) async-start(f32[16,5,512]{2,1,0:T(8,128)} %broadcast_in_dim.23), calls=%async_computation | async-start | bytes 524288 | tf_op jit(solution)/shard_map/all_to_all | solution.py:16
  29.8 15.1 %all-to-all-done = f32[16,5,512]{2,1,0:T(8,128)S(1)} async-done(((f32[16,5,512]{2,1,0:T(8,128)}), f32[16,5,512]{2,1,0:T(8,128)S(1)}, u32[]{:S(2)}, u32[]{:S(2)}) %all-to-all-start) | async-done | bytes 163872 | tf_op jit(solution)/shard_map/all_to_all | solution.py:16
  45.6 4.5 %all-to-all-start.1 = ((f32[4,5,512]{2,1,0:T(8,128)}), f32[4,5,512]{2,1,0:T(8,128)S(1)}, u32[]{:S(2)}, u32[]{:S(2)}) async-start(f32[4,5,512]{2,1,0:T(8,128)} %broadcast_in_dim.24), calls=%async_computation.1 | async-start | bytes 131072 | tf_op jit(solution)/shard_map/all_to_all | solution.py:16
  52.2 3.4 %all-to-all-done.1 = f32[4,5,512]{2,1,0:T(8,128)S(1)} async-done(((f32[4,5,512]{2,1,0:T(8,128)}), f32[4,5,512]{2,1,0:T(8,128)S(1)}, u32[]{:S(2)}, u32[]{:S(2)}) %all-to-all-start.1) | async-done | bytes 40992 | tf_op jit(solution)/shard_map/all_to_all | solution.py:16
  57.9 2.5 collective-permute-start
  60.4 4.6 %collective-permute-start.1 = (bf16[64,2048]{1,0:T(8,128)(2,1)}, bf16[64,2048]{1,0:T(8,128)(2,1)}, u32[]{:S(2)}, u32[]{:S(2)}) collective-permute-start(bf16[64,2048]{1,0:T(8,128)(2,1)} %get-tuple-element.126), channel_id=1, source_target_pairs={{0,24},{8,0},{16,8},{24,16},{1,25},{9,1},{17,9},{25,17},{2,26},{10... | collective-permute-start | bytes 786440 | tf_op jit(solution)/shard_map/ppermute | solution.py:188
  70.8 2.1 convolution_convert_fusion.1
  74.7 1.9 collective-permute-start.2
  77.7 6.5 %collective-permute-done.2 = bf16[64,2048]{1,0:T(8,128)(2,1)S(1)} collective-permute-done((bf16[64,2048]{1,0:T(8,128)(2,1)S(1)}, bf16[64,2048]{1,0:T(8,128)(2,1)S(1)}, u32[]{:S(2)}, u32[]{:S(2)}) %collective-permute-start.2) | collective-permute-done | bytes 262176 | tf_op jit(solution)/shard_map/ppermute | solution.py:183
  88.0 70.0 %all-gather.2.cloned.1.call-done = bf16[4352,512]{1,0:T(8,128)(2,1)} async-done(((bf16[272,512]{1,0:T(8,128)(2,1)}), bf16[4352,512]{1,0:T(8,128)(2,1)}) %all-gather.2.cloned.1.call-update) | async-done | bytes 4456464 | tf_op jit(solution)/shard_map/all_gather | solution.py:36
  158.0 1.6 fusion.42
  160.4 4.5 %fusion.43 = (bf16[4096,256]{1,0:T(8,128)(2,1)}, bf16[4096,256]{1,0:T(8,128)(2,1)}) fusion(bf16[4352,512]{1,0:T(8,128)(2,1)} %all-gather.2.cloned.1.call-done), kind=kLoop, calls=%fused_computation.106 | loop fusion | bytes 8388608 | tf_op jit(solution)/shard_map/slice | solution.py:125
  165.0 65.5 %while.13 = (s32[]{:T(128)}, f32[2,2,256,128]{2,3,0,1:T(8,128)}, f32[2,2,256]{2,1,0:T(2,128)S(1)}, bf16[8,512,256]{2,1,0:T(8,128)(2,1)}, bf16[8,512,256]{2,1,0:T...) while((s32[]{:T(128)}, f32[2,2,256,128]{2,3,0,1:T(8,128)}, ...), condition=%wide.region_8.9_spmd.clone, body=%wide.region_6.8_spmd.clone.sunk | while | flops 203686912 | bytes 10125424 | solution.py:135
  165.0 1.8 constant_dynamic-slice_fusion.3
  170.2 2.4 fusion.71
  173.0 1.8 constant_dynamic-slice_fusion.3
  178.3 2.6 fusion.71
  181.2 1.8 constant_dynamic-slice_fusion.3
  186.5 2.6 fusion.71
  189.4 1.8 constant_dynamic-slice_fusion.3
  194.7 2.6 fusion.71
  197.6 1.8 constant_dynamic-slice_fusion.3
  200.2 1.6 bitcast_convert_fusion.2
  202.9 2.6 fusion.71
  205.8 1.8 constant_dynamic-slice_fusion.3
  211.1 2.6 fusion.71
  214.0 1.8 constant_dynamic-slice_fusion.3
  219.3 2.6 fusion.71
  222.2 1.8 constant_dynamic-slice_fusion.3
  227.5 2.6 fusion.71
  235.0 21.2 %all_to_all.15 = f32[4,64,2048]{2,1,0:T(8,128)S(1)} all-to-all(f32[4,64,2048]{2,1,0:T(8,128)S(1)} %convolution_bitcast_fusion.1), channel_id=1, replica_groups=mesh['sp'=16,'tp'=4,'dp'=8] {'tp'}, dimensions={0} | all-to-all | bytes 4194304 | tf_op jit(solution)/shard_map/all_to_all | solution.py:50
  257.2 1.8 fusion.12
  (153 shorter events, 60.5 us)
Async XLA Ops:
  6.5 228.0 %copy-start = (bf16[256,2048]{1,0:T(8,128)(2,1)S(1)}, bf16[256,2048]{1,0:T(8,128)(2,1)}, u32[]{:S(2)}) copy-start(bf16[256,2048]{1,0:T(8,128)(2,1)} %param.35) | copy-start | bytes 3145732
  6.5 49.9 %copy-start.3 = (bf16[64,2048]{1,0:T(8,128)(2,1)S(1)}, bf16[64,2048]{1,0:T(8,128)(2,1)}, u32[]{:S(2)}) copy-start(bf16[64,2048]{1,0:T(8,128)(2,1)} %param.19) | copy-start | bytes 786436
  6.5 43.7 %copy-start.14 = (f32[64]{0:T(128)S(1)}, f32[64]{0:T(128)}, u32[]{:S(2)}) copy-start(f32[64]{0:T(128)} %param.31) | copy-start | bytes 772
  6.5 44.4 %copy-start.17 = (f32[64]{0:T(128)S(1)}, f32[64]{0:T(128)}, u32[]{:S(2)}) copy-start(f32[64]{0:T(128)} %param.30) | copy-start | bytes 772
  6.5 49.9 %copy-start.7 = (f32[2048]{0:T(1024)S(1)}, f32[2048]{0:T(1024)}, u32[]{:S(2)}) copy-start(f32[2048]{0:T(1024)} %param.23) | copy-start | bytes 24580
  8.4 56.6 %copy-start.1 = (bf16[2048,256]{1,0:T(8,128)(2,1)S(1)}, bf16[2048,256]{1,0:T(8,128)(2,1)}, u32[]{:S(2)}) copy-start(bf16[2048,256]{1,0:T(8,128)(2,1)} %param.28) | copy-start | bytes 3145732
  8.4 56.6 %copy-start.6 = (bf16[16,2048]{1,0:T(8,128)(2,1)S(1)}, bf16[16,2048]{1,0:T(8,128)(2,1)}, u32[]{:S(2)}) copy-start(bf16[16,2048]{1,0:T(8,128)(2,1)} %param.20) | copy-start | bytes 196612
  11.3 33.6 %all-to-all-start = ((f32[16,5,512]{2,1,0:T(8,128)}), f32[16,5,512]{2,1,0:T(8,128)S(1)}, u32[]{:S(2)}, u32[]{:S(2)}) async-start(f32[16,5,512]{2,1,0:T(8,128)} %broadcast_in_dim.23), calls=%async_computation | async-start | bytes 524288 | tf_op jit(solution)/shard_map/all_to_all | solution.py:16
  45.6 10.1 %all-to-all-start.1 = ((f32[4,5,512]{2,1,0:T(8,128)}), f32[4,5,512]{2,1,0:T(8,128)S(1)}, u32[]{:S(2)}, u32[]{:S(2)}) async-start(f32[4,5,512]{2,1,0:T(8,128)} %broadcast_in_dim.24), calls=%async_computation.1 | async-start | bytes 131072 | tf_op jit(solution)/shard_map/all_to_all | solution.py:16
  50.0 108.0 %all-gather.2.cloned.1.call-start = ((), (), s32[]{:S(2)}) async-start(), calls=%async_computation.3 | async-start | bytes 4734976 | tf_op jit(solution)/shard_map/all_gather | solution.py:36
  56.3 8.7 %copy-start.8 = (f32[1,4,512]{2,0,1:T(1,128)}, f32[1,4,512]{2,0,1:T(1,128)S(1)}, u32[]{:S(2)}) copy-start(f32[1,4,512]{2,0,1:T(1,128)S(1)} %get-tuple-element.143) | copy-start | bytes 24580
  57.9 16.8 %collective-permute-start = (bf16[64,2048]{1,0:T(8,128)(2,1)}, bf16[64,2048]{1,0:T(8,128)(2,1)S(1)}, u32[]{:S(2)}, u32[]{:S(2)}) collective-permute-start(bf16[64,2048]{1,0:T(8,128)(2,1)} %get-tuple-element.126), channel_id=1, source_target_pairs={{0,8},{8,16},{16,24},{24,0},{1,9},{9,17},{17,25},{25,1},{2,10},{10... | collective-permute-start | bytes 786440 | tf_op jit(solution)/shard_map/ppermute | solution.py:183
  60.4 16.3 %collective-permute-start.1 = (bf16[64,2048]{1,0:T(8,128)(2,1)}, bf16[64,2048]{1,0:T(8,128)(2,1)}, u32[]{:S(2)}, u32[]{:S(2)}) collective-permute-start(bf16[64,2048]{1,0:T(8,128)(2,1)} %get-tuple-element.126), channel_id=1, source_target_pairs={{0,24},{8,0},{16,8},{24,16},{1,25},{9,1},{17,9},{25,17},{2,26},{10... | collective-permute-start | bytes 786440 | tf_op jit(solution)/shard_map/ppermute | solution.py:188
  73.9 10.9 %copy-start.2 = (bf16[2048,256]{1,0:T(8,128)(2,1)S(1)}, bf16[2048,256]{1,0:T(8,128)(2,1)}, u32[]{:S(2)}) copy-start(bf16[2048,256]{1,0:T(8,128)(2,1)} %param.29) | copy-start | bytes 3145732
  74.7 9.5 %collective-permute-start.2 = (bf16[64,2048]{1,0:T(8,128)(2,1)S(1)}, bf16[64,2048]{1,0:T(8,128)(2,1)S(1)}, u32[]{:S(2)}, u32[]{:S(2)}) collective-permute-start(bf16[64,2048]{1,0:T(8,128)(2,1)S(1)} %collective-permute-done), channel_id=1, source_target_pairs={{0,8},{8,16},{16,24},{24,0},{1,9},{9,17},{17,25},{25,1},{2,10},{10... | collective-permute-start | bytes 786440 | tf_op jit(solution)/shard_map/ppermute | solution.py:183
  84.2 1.2 copy-start.5
  84.8 1.3 copy-start.12
  84.8 1.3 copy-start.11
  85.5 1.0 copy-start.9
  86.0 1.2 copy-start.15
  230.5 3.7 %copy-start.13 = (f32[2]{0:T(128)S(1)}, f32[2]{0:T(128)}, u32[]{:S(2)}) copy-start(f32[2]{0:T(128)} %param.32) | copy-start | bytes 28
  230.5 3.8 %copy-start.16 = (f32[128]{0:T(128)S(1)}, f32[128]{0:T(128)}, u32[]{:S(2)}) copy-start(f32[128]{0:T(128)} %param.34) | copy-start | bytes 1540
  256.2 1.0 copy-start.4
  256.2 1.0 copy-start.10
Sparse Core Ops, SparseCore 0:
  87.3 70.6 all-gather.1
